TPU v7x, 32 devices: a whole 2x2x4 slice. The times are simulated.
32 devices in a mesh: sp: 8 (over z, y), tp: 4 (over x, core).
Axes of the slice: x: 2, y: 2, z: 4, core: 2. Of those that a mesh axis runs over, the one named last changes fastest.
Arguments:
- prompt_input: bfloat16 [2304, 2048], P('sp'), may hold values from -6 to 6
- next_input: bfloat16 [2048], replicated, may hold values from -6 to 6
- norm_gain: float32 [2048], replicated, may hold values from 0.1 to 1.9
- w_key: bfloat16 [2048, 1024], P(None, 'tp'), may hold values from -0.125 to 0.125
- w_value: bfloat16 [2048, 1024], P(None, 'tp'), may hold values from -0.125 to 0.125
- w_query: bfloat16 [2048, 1024], P(None, 'tp'), may hold values from -0.125 to 0.125
- key_offset: float32 [2304, 8], P('sp', 'tp'), may hold values from -10 to 0, as said below
Outputs:
- key_cache: bfloat16 [8, 8, 36, 1024], P('sp', None, None, 'tp')
- value_cache: bfloat16 [8, 8, 36, 1024], P('sp', None, None, 'tp')
- reading: bfloat16 [1024], replicated
Inputs may be any that keep to these rules, and one draw needn't show every extreme that they name: `key_offset`: finite log-odds offsets, one per key and head.
All inputs are finite; a program needn't handle non-finite values.
Results may differ from a plain program's by a relative error of at most 0.011.
Values may be sent and summed in bfloat16 or wider, within the bound.
A program may use at most 64 MiB of HBM per device.

v0:
```python
import jax
import jax.numpy as jnp
from jax import lax
from jax.sharding import PartitionSpec as P

HEAD_DIM = 128


def norm_rows(row_block, gain_vec):
    wide_rows = row_block.astype(jnp.float32)
    inv_rms = lax.rsqrt(jnp.mean(wide_rows * wide_rows, axis=-1, keepdims=True) + 1e-06)
    return (wide_rows * inv_rms * gain_vec).astype(jnp.bfloat16)


def shards(prompt_input, next_input, norm_gain, w_key, w_value, w_query, key_offset):
    span_len = prompt_input.shape[0]
    head_width = w_key.shape[1]
    heads_here = head_width // HEAD_DIM
    score_scale = HEAD_DIM ** (-0.5)
    slots = lax.axis_size("sp")
    sub_len = span_len // slots
    normed = norm_rows(prompt_input, norm_gain)
    key_rows = jnp.dot(normed, w_key, preferred_element_type=jnp.float32).astype(jnp.bfloat16)
    value_rows = jnp.dot(normed, w_value, preferred_element_type=jnp.float32).astype(jnp.bfloat16)
    outgoing = jnp.stack([key_rows, value_rows]).reshape(2, slots, 1, sub_len, head_width)
    arrived = lax.all_to_all(outgoing, "sp", split_axis=1, concat_axis=2, tiled=True)
    key_cache = arrived[0]
    value_cache = arrived[1]
    new_query = jnp.dot(
        norm_rows(next_input[None, :], norm_gain), w_query, preferred_element_type=jnp.float32
    )
    new_query = new_query.astype(jnp.bfloat16).reshape(heads_here, HEAD_DIM)
    key_heads = key_rows.reshape(span_len, heads_here, HEAD_DIM)
    value_heads = value_rows.reshape(span_len, heads_here, HEAD_DIM)
    logits = (
        jnp.einsum("hd,shd->sh", new_query, key_heads, preferred_element_type=jnp.float32)
        * score_scale
        + key_offset
    )
    log_breaks = jax.nn.log_sigmoid(-logits)
    inner_sum = lax.cumsum(log_breaks, axis=0, reverse=True) - log_breaks
    block_totals = jnp.sum(log_breaks, axis=0)
    every_total = lax.all_gather(block_totals[None], "sp", axis=0, tiled=True)
    block_ids = lax.broadcasted_iota(jnp.int32, every_total.shape, 0)
    carried = jnp.sum(jnp.where(block_ids > lax.axis_index("sp"), every_total, 0.0), axis=0)
    weights = jnp.exp(jax.nn.log_sigmoid(logits) + inner_sum + carried[None, :])
    partial_value = jnp.einsum("sh,shd->hd", weights, value_heads.astype(jnp.float32))
    summed = lax.psum(partial_value, "sp")
    own_read = summed.reshape(head_width).astype(jnp.bfloat16)
    reading = lax.all_gather(own_read, "tp", axis=0, tiled=True)
    return (key_cache, value_cache, reading)


def solution(mesh):
    placed = (P("sp", None), P(), P(), P(None, "tp"), P(None, "tp"), P(None, "tp"), P("sp", "tp"))
    return jax.shard_map(
        shards,
        mesh=mesh,
        in_specs=placed,
        out_specs=(P("sp", None, None, "tp"), P("sp", None, None, "tp"), P()),
        check_vma=False,
    )
```

profile of v0, /device:TPU:0, one launch (start us, length us, event | category | flops | bytes accessed | tf_op | source)
XLA Modules:
  0.0 65.4 jit_solution(9334492287471043287)
XLA Ops:
  0.6 0.0 copy-start
  0.7 1.7 %fusion = f32[288]{0:T(512)S(1)} fusion(bf16[288,2048]{1,0:T(8,128)(2,1)} %param.7), kind=kLoop, calls=%fused_computation.2 | loop fusion | flops 1769184 | bytes 1180800 | tf_op jit(solution)/shard_map/reduce_sum | solution.py:11
  2.4 0.2 copy-done.1
  2.6 1.3 %convolution_convert_fusion = bf16[288,256]{1,0:T(8,128)(2,1)S(1)} fusion(bf16[2048,256]{1,0:T(8,128)(2,1)S(1)} %copy-done, bf16[288,2048]{1,0:T(8,128)(2,1)S(1)} %copy-done.1, f32[2048]{0:T(1024)} %param.9, f32[288]{0:T(512)S(1)} %add_rsqrt_fusion), kind=kOutput, calls=%fused_computation.5 | convolution fusion | flops 304422912 | bytes 2385024 | tf_op jit(solution)/shard_map/dot_general | solution.py:24
  3.9 0.5 convolution_convert_fusion.1
  4.5 0.0 copy-start.3
  4.5 0.0 copy-start.2
  4.6 0.0 copy-start.7
  4.6 0.0 copy-start.4
  4.6 1.0 %copy.17 = bf16[2,8,1,36,256]{4,0,3,2,1:T(2,128)(2,1)} copy(bf16[2,8,1,36,256]{4,3,1,2,0:T(8,128)(2,1)S(1)} %pad_maximum_fusion) | data formatting | bytes 589824 | tf_op jit(solution)/shard_map/stack | solution.py:25
  5.6 7.3 %all-to-all-start = ((bf16[2,8,1,36,256]{4,0,3,2,1:T(2,128)(2,1)}), bf16[2,8,1,36,256]{4,0,3,2,1:T(2,128)(2,1)S(1)}, u32[]{:S(2)}, u32[]{:S(2)}) async-start(bf16[2,8,1,36,256]{4,0,3,2,1:T(2,128)(2,1)} %copy.17), calls=%async_computation | async-start | bytes 589824 | tf_op jit(solution)/shard_map/all_to_all | solution.py:26
  13.0 0.6 fusion.11
  14.3 0.2 fusion.21
  14.5 0.1 fusion.8
  14.7 0.6 dynamic-slice
  16.0 0.1 fusion.19
  16.1 0.1 negate_dynamic-update-slice_fusion
  16.2 21.8 %all-reduce.1 = f32[16]{0:T(128)S(1)} all-reduce(f32[16]{0:T(128)S(1)} %negate_dynamic-update-slice_fusion), channel_id=2, replica_groups=mesh['sp'=8,'tp'=4] {'sp'}, use_global_device_ids=true, to_apply=%add.1 | all-reduce | flops 16 | bytes 128
  38.1 2.5 %reduce-window.6 = f32[2,3,128]{2,1,0:T(4,128)S(1)} reduce-window(f32[2,3,128]{2,1,0:T(4,128)S(1)} %reshape.81, f32[]{:T(128)} %constant.20.clone.1), window={size=1x1x128 pad=0_0x0_0x0_127}, to_apply=%region_2.3 | reduce-window | flops 97536 | bytes 6148 | tf_op jit(solution)/shard_map/reduce-window
  40.6 0.1 slice_reduce_fusion
  40.7 0.2 reduce-window.9
  40.9 0.1 slice.21
  40.9 0.1 add_bitcast_fusion
  41.0 0.1 reshape.84
  41.1 0.1 select_reduce_fusion
  41.2 0.1 exponential_bitcast_fusion
  41.3 0.1 fusion.5
  41.4 17.1 %psum.7 = bf16[2,128]{1,0:T(2,128)(2,1)S(1)} all-reduce(f32[2,128]{1,0:T(2,128)S(1)} %bitcast.64), channel_id=1, replica_groups=mesh['sp'=8,'tp'=4] {'sp'}, use_global_device_ids=true, to_apply=%region_6.7 | all-reduce | flops 256 | bytes 1536 | tf_op jit(solution)/shard_map/psum | solution.py:48
  58.6 5.1 %all-gather.1 = bf16[4,1,256]{2,1,0:T(2,128)(2,1)S(1)} all-gather(bf16[1,1,256]{2,1,0:T(2,128)(2,1)S(1)} %reshape.88), channel_id=1, replica_groups=mesh['sp'=8,'tp'=4] {'tp'}, dimensions={0}, use_global_device_ids=true | all-gather | bytes 2560 | tf_op jit(solution)/shard_map/all_gather | solution.py:50
  63.6 0.6 copy.31
  64.2 0.4 fusion.20
  64.6 0.8 %copy_bitcast_fusion = (bf16[1,8,36,256]{3,1,2,0:T(8,128)(2,1)}, bf16[1,8,36,256]{3,1,2,0:T(8,128)(2,1)}) fusion(bf16[1,8,1,36,256]{4,0,3,2,1:T(2,128)(2,1)S(1)} %get-tuple-element.11, bf16[1,8,1,36,256]{4,0,3,2,1:T(2,128)(2,1)S(1)} %get-tuple-element.12), kind=kLoop, calls=%fused_computation.14 | loop fusion | bytes 589824 | tf_op jit(solution)/shard_map/squeeze | solution.py:28
  (26 shorter events, 0.2 us)
Async XLA Ops:
  0.6 1.8 %copy-start = (bf16[2048,256]{1,0:T(8,128)(2,1)S(1)}, bf16[2048,256]{1,0:T(8,128)(2,1)}, u32[]{:S(2)}) copy-start(bf16[2048,256]{1,0:T(8,128)(2,1)} %param.11) | copy-start | bytes 3145732
  0.6 1.9 %copy-start.1 = (bf16[288,2048]{1,0:T(8,128)(2,1)S(1)}, bf16[288,2048]{1,0:T(8,128)(2,1)}, u32[]{:S(2)}) copy-start(bf16[288,2048]{1,0:T(8,128)(2,1)} %param.7) | copy-start | bytes 3538948
  2.6 1.3 %copy-start.5 = (f32[2048]{0:T(1024)S(1)}, f32[2048]{0:T(1024)}, u32[]{:S(2)}) copy-start(f32[2048]{0:T(1024)} %param.9) | copy-start | bytes 24580
  2.6 1.3 %copy-start.6 = (bf16[2048,256]{1,0:T(8,128)(2,1)S(1)}, bf16[2048,256]{1,0:T(8,128)(2,1)}, u32[]{:S(2)}) copy-start(bf16[2048,256]{1,0:T(8,128)(2,1)} %param.10) | copy-start | bytes 3145732
  4.5 8.5 %copy-start.3 = (bf16[2048]{0:T(1024)(128)(2,1)S(1)}, bf16[2048]{0:T(1024)(128)(2,1)}, u32[]{:S(2)}) copy-start(bf16[2048]{0:T(1024)(128)(2,1)} %param.8) | copy-start | bytes 12292
  4.5 9.8 %copy-start.2 = (bf16[2048,256]{1,0:T(8,128)(2,1)S(1)}, bf16[2048,256]{1,0:T(8,128)(2,1)}, u32[]{:S(2)}) copy-start(bf16[2048,256]{1,0:T(8,128)(2,1)} %param.12) | copy-start | bytes 3145732
  4.6 10.1 %copy-start.7 = (u32[32]{0:T(128)S(1)}, u32[32]{0:T(128)}, u32[]{:S(2)}) copy-start(u32[32]{0:T(128)} %constant.31) | copy-start | bytes 388
  4.6 11.3 %copy-start.4 = (f32[288,2]{0,1:T(2,128)S(1)}, f32[288,2]{0,1:T(2,128)}, u32[]{:S(2)}) copy-start(f32[288,2]{0,1:T(2,128)} %param.13) | copy-start | bytes 6916
  5.6 58.6 %all-to-all-start = ((bf16[2,8,1,36,256]{4,0,3,2,1:T(2,128)(2,1)}), bf16[2,8,1,36,256]{4,0,3,2,1:T(2,128)(2,1)S(1)}, u32[]{:S(2)}, u32[]{:S(2)}) async-start(bf16[2,8,1,36,256]{4,0,3,2,1:T(2,128)(2,1)} %copy.17), calls=%async_computation | async-start | bytes 589824 | tf_op jit(solution)/shard_map/all_to_all | solution.py:26
where the time goes:
time: 65.7 us; the launch traced here: 65.4 us
  blocking collectives  44 us (67%)
  starting transfers between devices  7.31 us (11%)
  other arithmetic  5.61 us (9%)
  local copies, waits for them, and re-layouts  3.98 us (6%)
  matrix products  2.36 us (4%)
  between operations  2.15 us (3%)
    unnamed x1, blocking collectives  21.8 us
    psum x1, blocking collectives, shards(): summed = lax.psum(partial_value, 'sp')  17.1 us
    all_to_all x1, starting transfers between devices, shards(): lax.all_to_all(outgoing, 'sp', split_axis=1, concat_axis=2, tiled=True)  7.31 us
    all_gather x1, blocking collectives, shards(): reading = lax.all_gather(own_read, 'tp', axis=0, tiled=True)  5.05 us
    another operation x2, other arithmetic  2.71 us
    reduce_sum x2, other arithmetic, norm_rows(): jnp.mean(wide_rows * wide_rows, axis=-1, keepdims=True) + 1e-06  2.34 us
    unnamed x21, local copies, waits for them, and re-layouts  1.43 us
  transfers between devices with their start and end apart: 1, of which 0 were waited for; matrix products, arithmetic and copies ran while one was open for 9% of the time, Pallas kernels for 0%

commit v1 on v0

--- a/solution.py
+++ b/solution.py
@@ -23,7 +23,16 @@
     key_rows = jnp.dot(normed, w_key, preferred_element_type=jnp.float32).astype(jnp.bfloat16)
     value_rows = jnp.dot(normed, w_value, preferred_element_type=jnp.float32).astype(jnp.bfloat16)
     outgoing = jnp.stack([key_rows, value_rows]).reshape(2, slots, 1, sub_len, head_width)
-    arrived = lax.all_to_all(outgoing, "sp", split_axis=1, concat_axis=2, tiled=True)
+    _do_sheet = lambda frame: jnp.concatenate(
+        jax.lax.all_to_all(
+            jnp.stack(jnp.split(frame, jax.lax.axis_size("sp"), axis=1), axis=0),
+            axis_name="sp",
+            split_axis=0,
+            concat_axis=0,
+        ),
+        axis=2,
+    )
+    arrived = _do_sheet(outgoing)
     key_cache = arrived[0]
     value_cache = arrived[1]
     new_query = jnp.dot(

time: 65.7 us -> 65.4 us (level)
    another operation x3, local copies, waits for them, and re-layouts: 1.07 us -> 0.08 us  [shards(): jnp.stack([key_rows, value_rows]).reshape(2, slots, 1, sub_len, head_width)]
    another operation x1 -> x3, local copies, waits for them, and re-layouts: 0.07 us -> 1.01 us  [the longest x2 0.94 us: shards(): jnp.stack(jnp.split(frame, jax.lax.axis_size('sp'), axis=1), axis=0)]
    unnamed x21 -> x29, local copies, waits for them, and re-layouts: 1.43 us -> 1.47 us
    another operation x3 -> x2, other arithmetic: 2.74 us -> 2.71 us
where the time goes in v1:
time: 65.4 us; the launch traced here: 65 us
  blocking collectives  44 us (67%)
  starting transfers between devices  7.31 us (11%)
  other arithmetic  5.57 us (9%)
  local copies, waits for them, and re-layouts  3.55 us (5%)
  matrix products  2.35 us (4%)
  between operations  2.22 us (3%)
    unnamed x1, blocking collectives  21.8 us
    psum x1, blocking collectives, shards(): summed = lax.psum(partial_value, 'sp')  17.1 us
    all_to_all x1, starting transfers between devices, shards(): jax.lax.all_to_all(jnp.stack(jnp.split(frame, jax.lax.axis_size('sp'), ax...  7.31 us
    all_gather x1, blocking collectives, shards(): reading = lax.all_gather(own_read, 'tp', axis=0, tiled=True)  5.05 us
    another operation x2, other arithmetic  2.71 us
    reduce_sum x2, other arithmetic, norm_rows(): jnp.mean(wide_rows * wide_rows, axis=-1, keepdims=True) + 1e-06  2.34 us
    unnamed x29, local copies, waits for them, and re-layouts  1.47 us
  transfers between devices with their start and end apart: 1, of which 0 were waited for; matrix products, arithmetic and copies ran while one was open for 9% of the time, Pallas kernels for 0%

profile of v1, /device:TPU:0, one launch (start us, length us, event | category | flops | bytes accessed | tf_op | source)
XLA Modules:
  0.0 65.0 jit_solution(1854407238710494728)
XLA Ops:
  0.6 0.0 copy-start
  0.7 1.7 %fusion = f32[288]{0:T(512)S(1)} fusion(bf16[288,2048]{1,0:T(8,128)(2,1)} %param.7), kind=kLoop, calls=%fused_computation.2 | loop fusion | flops 1769184 | bytes 1180800 | tf_op jit(solution)/shard_map/reduce_sum | solution.py:11
  2.4 0.2 copy-done.1
  2.6 1.3 %convolution_convert_fusion = bf16[288,256]{1,0:T(8,128)(2,1)S(1)} fusion(bf16[2048,256]{1,0:T(8,128)(2,1)S(1)} %copy-done, bf16[288,2048]{1,0:T(8,128)(2,1)S(1)} %copy-done.1, f32[2048]{0:T(1024)} %param.9, f32[288]{0:T(512)S(1)} %add_rsqrt_fusion), kind=kOutput, calls=%fused_computation.5 | convolution fusion | flops 304422912 | bytes 2385024 | tf_op jit(solution)/shard_map/dot_general | solution.py:24
  3.9 0.5 convolution_convert_fusion.1
  4.6 0.0 copy-start.3
  4.6 0.0 copy-start.2
  4.7 0.0 copy-start.7
  4.7 0.0 copy-start.4
  4.7 0.9 %copy.48 = bf16[8,2,1,1,36,256]{5,1,4,3,2,0:T(2,128)(2,1)} copy(bf16[8,2,1,1,36,256]{5,4,1,3,2,0:T(8,128)(2,1)S(1)} %fusion.11) | data formatting | bytes 589824 | tf_op jit(solution)/shard_map/stack | solution.py:28
  5.7 7.3 %all-to-all-start = ((bf16[8,2,1,1,36,256]{5,1,4,3,2,0:T(2,128)(2,1)}), bf16[8,2,1,1,36,256]{5,1,4,3,2,0:T(2,128)(2,1)S(1)}, u32[]{:S(2)}, u32[]{:S(2)}) async-start(bf16[8,2,1,1,36,256]{5,1,4,3,2,0:T(2,128)(2,1)} %copy.48), calls=%async_computation | async-start | bytes 589824 | tf_op jit(solution)/shard_map/all_to_all | solution.py:27
  13.0 0.6 fusion.19
  14.3 0.2 fusion.28
  14.6 0.1 fusion.8
  14.7 0.6 dynamic-slice
  16.0 0.1 fusion.27
  16.1 0.1 negate_dynamic-update-slice_fusion
  16.2 21.8 %all-reduce.1 = f32[16]{0:T(128)S(1)} all-reduce(f32[16]{0:T(128)S(1)} %negate_dynamic-update-slice_fusion), channel_id=2, replica_groups=mesh['sp'=8,'tp'=4] {'sp'}, use_global_device_ids=true, to_apply=%add.1 | all-reduce | flops 16 | bytes 128
  38.1 2.5 %reduce-window.6 = f32[2,3,128]{2,1,0:T(4,128)S(1)} reduce-window(f32[2,3,128]{2,1,0:T(4,128)S(1)} %reshape.81, f32[]{:T(128)} %constant.20.clone.1), window={size=1x1x128 pad=0_0x0_0x0_127}, to_apply=%region_2.3 | reduce-window | flops 97536 | bytes 6148 | tf_op jit(solution)/shard_map/reduce-window
  40.6 0.1 slice_reduce_fusion
  40.7 0.2 reduce-window.9
  40.9 0.1 slice.20
  41.0 0.1 add_bitcast_fusion
  41.0 0.1 reshape.84
  41.1 0.1 select_reduce_fusion
  41.2 0.1 exponential_bitcast_fusion
  41.3 0.1 fusion.5
  41.4 17.1 %psum.7 = bf16[2,128]{1,0:T(2,128)(2,1)S(1)} all-reduce(f32[2,128]{1,0:T(2,128)S(1)} %bitcast.112), channel_id=1, replica_groups=mesh['sp'=8,'tp'=4] {'sp'}, use_global_device_ids=true, to_apply=%region_6.7 | all-reduce | flops 256 | bytes 1536 | tf_op jit(solution)/shard_map/psum | solution.py:57
  58.6 5.1 %all-gather.1 = bf16[4,1,256]{2,1,0:T(2,128)(2,1)S(1)} all-gather(bf16[1,1,256]{2,1,0:T(2,128)(2,1)S(1)} %reshape.88), channel_id=1, replica_groups=mesh['sp'=8,'tp'=4] {'tp'}, dimensions={0}, use_global_device_ids=true | all-gather | bytes 2560 | tf_op jit(solution)/shard_map/all_gather | solution.py:59
  63.7 0.6 copy.66
  64.2 0.1 copy.87
  64.3 0.7 %slice_bitcast_fusion = (bf16[1,8,36,256]{3,1,2,0:T(8,128)(2,1)}, bf16[1,8,36,256]{3,1,2,0:T(8,128)(2,1)}) fusion(bf16[2,1,8,1,36,256]{5,2,4,3,1,0:T(8,128)(2,1)S(1)} %bitcast.107), kind=kLoop, calls=%fused_computation.14 | loop fusion | bytes 589824 | tf_op jit(solution)/shard_map/squeeze | solution.py:37
  (35 shorter events, 0.3 us)
Async XLA Ops:
  0.6 1.8 %copy-start = (bf16[2048,256]{1,0:T(8,128)(2,1)S(1)}, bf16[2048,256]{1,0:T(8,128)(2,1)}, u32[]{:S(2)}) copy-start(bf16[2048,256]{1,0:T(8,128)(2,1)} %param.11) | copy-start | bytes 3145732
  0.6 1.9 %copy-start.1 = (bf16[288,2048]{1,0:T(8,128)(2,1)S(1)}, bf16[288,2048]{1,0:T(8,128)(2,1)}, u32[]{:S(2)}) copy-start(bf16[288,2048]{1,0:T(8,128)(2,1)} %param.7) | copy-start | bytes 3538948
  2.6 1.3 %copy-start.5 = (f32[2048]{0:T(1024)S(1)}, f32[2048]{0:T(1024)}, u32[]{:S(2)}) copy-start(f32[2048]{0:T(1024)} %param.9) | copy-start | bytes 24580
  2.6 1.3 %copy-start.6 = (bf16[2048,256]{1,0:T(8,128)(2,1)S(1)}, bf16[2048,256]{1,0:T(8,128)(2,1)}, u32[]{:S(2)}) copy-start(bf16[2048,256]{1,0:T(8,128)(2,1)} %param.10) | copy-start | bytes 3145732
  4.6 8.4 %copy-start.3 = (bf16[2048]{0:T(1024)(128)(2,1)S(1)}, bf16[2048]{0:T(1024)(128)(2,1)}, u32[]{:S(2)}) copy-start(bf16[2048]{0:T(1024)(128)(2,1)} %param.8) | copy-start | bytes 12292
  4.6 9.7 %copy-start.2 = (bf16[2048,256]{1,0:T(8,128)(2,1)S(1)}, bf16[2048,256]{1,0:T(8,128)(2,1)}, u32[]{:S(2)}) copy-start(bf16[2048,256]{1,0:T(8,128)(2,1)} %param.12) | copy-start | bytes 3145732
  4.7 10.0 %copy-start.7 = (u32[32]{0:T(128)S(1)}, u32[32]{0:T(128)}, u32[]{:S(2)}) copy-start(u32[32]{0:T(128)} %constant.31) | copy-start | bytes 388
  4.7 11.3 %copy-start.4 = (f32[288,2]{0,1:T(2,128)S(1)}, f32[288,2]{0,1:T(2,128)}, u32[]{:S(2)}) copy-start(f32[288,2]{0,1:T(2,128)} %param.13) | copy-start | bytes 6916
  5.7 58.6 %all-to-all-start = ((bf16[8,2,1,1,36,256]{5,1,4,3,2,0:T(2,128)(2,1)}), bf16[8,2,1,1,36,256]{5,1,4,3,2,0:T(2,128)(2,1)S(1)}, u32[]{:S(2)}, u32[]{:S(2)}) async-start(bf16[8,2,1,1,36,256]{5,1,4,3,2,0:T(2,128)(2,1)} %copy.48), calls=%async_computation | async-start | bytes 589824 | tf_op jit(solution)/shard_map/all_to_all | solution.py:27
